TPU v7x, 512 devices: a 8x2x16 block of a 8x8x16 slice. The times are simulated.
512 devices in a mesh: grp: 2 (over y), ep: 32 (over z, core), tp: 8 (over x).
Axes of the slice: x: 8, y: 2, z: 16, core: 2. Of those that a mesh axis runs over, the one named last changes fastest.
The devices are a block of a 8x8x16 slice.
Arguments:
- tokens: bfloat16 [16384, 2048], P(('grp', 'ep'), 'tp'), parts along dimension 0, may hold values from -6 to 6
- norm_gain: float32 [2048], replicated, may hold values from 0.1 to 1.9
- expert_ids: int32 [16384, 2], P(('grp', 'ep')), parts along dimension 0, may hold values from 0 to 31, all different within a row; in each aligned block of 256 rows (0 to 255, 256 to 511, ...) at most 24 rows name the same one
- gate_weights: float32 [16384, 2], P(('grp', 'ep')), parts along dimension 0, may hold values from 0.25 to 1
- w_gate: bfloat16 [32, 2048, 3072], P('ep', None, 'tp'), may hold values from -0.125 to 0.125
- w_up: bfloat16 [32, 2048, 3072], P('ep', None, 'tp'), may hold values from -0.125 to 0.125
- w_down: bfloat16 [32, 3072, 2048], P('ep', 'tp'), may hold values from -0.15625 to 0.15625
Outputs:
- mixed: bfloat16 [16384, 2048], P(('grp', 'ep'), 'tp'), parts along dimension 0
There are 2 independent parts, one for each index of `grp`. A program takes and returns all parts, laid end to end along the dimension named above; an argument that names none is the same for every part. Nothing has to cross between parts.
Inputs may be any that keep to these rules, and one draw needn't show every extreme that they name: `expert_ids`: each token names 2 different experts. Within the 256 rows of one index of ep (aligned blocks) no expert is named more than 24 times, and in some blocks one expert is named exactly 24 times.
All inputs are finite; a program needn't handle non-finite values.
Results may differ from a plain program's by a relative error of at most 0.015.
Values may be sent and summed in bfloat16 or wider, within the bound.
A program may use at most 64 MiB of HBM per device.

v0:
```python
import jax
import jax.numpy as jnp
from jax import lax
from jax.sharding import Mesh
from jax.sharding import PartitionSpec as P

EP = ("ep_0", "ep_1")
GRP_EP = ("grp", "ep_0", "ep_1")
epsilon = 1e-06


def sent_to_all(array, axis):
    count = lax.axis_size(axis)
    return lax.all_to_all(
        jnp.broadcast_to(array[None], (count, *array.shape)), axis, 0, 0, tiled=True
    )


def over_copies(array, axis):
    everything = sent_to_all(array, axis)
    return jnp.sum(everything, axis=0)


def in_blocks(array, dim, count):
    dims = array.shape
    blocks = array.reshape(*dims[:dim], count, dims[dim] // count, *dims[dim + 1 :])
    return jnp.moveaxis(blocks, dim, 0)


def joined_along(blocks, dim):
    dims = list(blocks.shape[1:])
    dims[dim] *= blocks.shape[0]
    return jnp.moveaxis(blocks, 0, dim).reshape(dims)


def moved_by_axis(blocks, axes, order):
    inside = blocks.shape[1:]
    whole = blocks.reshape(*(lax.axis_size(a) for a in axes), *inside)
    for k in order:
        whole = lax.all_to_all(whole, axes[k], k, k, tiled=True)
    return whole.reshape(-1, *inside)


def core_and_chips(array, groups, order, split_dim, concat_dim):
    count = lax.axis_size(groups[0]) * lax.axis_size(groups[1])
    blocks = in_blocks(array, split_dim, count)
    return joined_along(moved_by_axis(blocks, groups, order), concat_dim)


def on_device(tokens, norm_gain, expert_ids, gate_weights, w_gate, w_up, w_down):
    tok_count = tokens.shape[0]
    top_count = expert_ids.shape[1]
    expert_count = lax.axis_size(EP)
    capacity = 3 * tok_count * top_count // (2 * expert_count)
    model_width = norm_gain.shape[0]
    flat_ids = expert_ids.reshape(-1)
    onehot = (flat_ids[:, None] == jnp.arange(expert_count, dtype=jnp.int32)[None, :]).astype(
        jnp.int32
    )
    earlier = jnp.cumsum(onehot, axis=0) - onehot
    slot_index = jnp.sum(earlier * onehot, axis=1)
    dest_index = flat_ids * capacity + slot_index
    owner_index = jnp.arange(tok_count * top_count, dtype=jnp.int32) // top_count
    slot_token = (
        jnp.full((expert_count * capacity,), tok_count, jnp.int32).at[dest_index].set(owner_index)
    )
    tok_values = tokens.astype(jnp.float32)
    square_sum = over_copies(jnp.sum(tok_values * tok_values, axis=1, keepdims=True), "tp")
    col_count = tokens.shape[1]
    gain_part = lax.dynamic_slice_in_dim(norm_gain, lax.axis_index("tp") * col_count, col_count)
    normed = (tok_values * lax.rsqrt(square_sum / model_width + epsilon) * gain_part).astype(
        jnp.bfloat16
    )
    buffer = jnp.take(normed, slot_token, axis=0, mode="fill", fill_value=0).reshape(
        expert_count, capacity, -1
    )
    received = core_and_chips(buffer, ("ep_0", "ep_1"), (1, 0), 0, 0)
    source_count, item_count, col_count = received.shape
    tok_rows = received.reshape(-1, col_count)
    col_piece = lax.all_gather(tok_rows, "tp", axis=1, tiled=True)
    gate_rows = w_gate[0]
    up_rows = w_up[0]
    gate_part = jnp.dot(col_piece, gate_rows, preferred_element_type=jnp.float32)
    up_part = jnp.dot(col_piece, up_rows, preferred_element_type=jnp.float32)
    hidden = (jax.nn.silu(gate_part) * up_part).astype(jnp.bfloat16)
    partial_value = jnp.dot(hidden, w_down[0], preferred_element_type=jnp.float32)
    partial_value = partial_value.reshape(source_count, item_count, -1)
    summed = lax.psum_scatter(
        partial_value.astype(jnp.bfloat16), "tp", scatter_dimension=2, tiled=True
    )
    came_back = lax.all_to_all(summed, EP, split_axis=0, concat_axis=0, tiled=True)
    picked = came_back.reshape(expert_count * capacity, -1)[dest_index].astype(jnp.float32)
    weighted = picked * gate_weights.reshape(-1)[:, None]
    return jnp.sum(weighted.reshape(tok_count, top_count, -1), axis=1).astype(jnp.bfloat16)


def solution(mesh):
    finer = Mesh(
        mesh.devices.reshape(mesh.shape["grp"], 16, 2, mesh.shape["tp"]),
        ("grp", "ep_0", "ep_1", "tp"),
    )
    in_specs = (
        P(GRP_EP, "tp"),
        P(),
        P(GRP_EP, None),
        P(GRP_EP, None),
        P(EP, None, "tp"),
        P(EP, None, "tp"),
        P(EP, "tp", None),
    )
    out_specs = P(GRP_EP, "tp")
    return jax.shard_map(
        on_device, mesh=finer, in_specs=in_specs, out_specs=out_specs, check_vma=False
    )
```

profile of v0, /device:TPU:65, one launch (start us, length us, event | category | flops | bytes accessed | tf_op | source)
XLA Modules:
  0.0 271.2 jit_solution(14151282188558710371)
XLA Ops:
  6.6 1.1 fusion.11
  7.7 0.6 broadcast_in_dim.29
  8.3 7.9 %all-to-all-start = ((f32[8,256,1]{1,2,0:T(1,128)}), f32[8,256,1]{1,2,0:T(1,128)S(1)}, u32[]{:S(2)}, u32[]{:S(2)}) async-start(f32[8,256,1]{1,2,0:T(1,128)} %broadcast_in_dim.29), calls=%async_computation | async-start | bytes 16384 | tf_op jit(solution)/shard_map/all_to_all | solution.py:14
  16.2 0.8 copy.15
  17.0 0.1 eq.29
  17.2 0.1 eq.25
  17.3 0.7 broadcast_multiply_fusion
  18.0 1.2 reduce-window.6
  19.2 0.2 slice_reduce_fusion
  19.5 0.1 copy.14
  19.6 0.1 mul.59
  19.8 0.1 fusion.16
  19.9 2.4 scatter_custom_fusion
  22.4 0.1 broadcast_in_dim.27
  22.5 0.8 dynamic_slice.3
  23.3 1.0 fusion.13
  24.3 2.7 gather_fusion
  27.0 0.2 copy_select_fusion
  27.2 41.3 %all_to_all.20 = bf16[16,2,1,24,256]{4,3,0,2,1:T(8,128)(2,1)S(1)} all-to-all(bf16[16,2,1,24,256]{4,3,0,2,1:T(8,128)(2,1)S(1)} %copy_select_fusion), channel_id=1, replica_groups=mesh['grp'=2,'ep_0'=16,'ep_1'=2,'tp'=8] {'ep_1'}, dimensions={1} | all-to-all | bytes 786432 | tf_op jit(solution)/shard_map/all_to_all | solution.py:40
  68.5 24.6 %all_to_all.21 = bf16[16,2,1,24,256]{4,3,1,2,0:T(8,128)(2,1)} all-to-all(bf16[16,2,1,24,256]{4,3,1,2,0:T(8,128)(2,1)S(1)} %copy.20), channel_id=1, replica_groups=mesh['grp'=2,'ep_0'=16,'ep_1'=2,'tp'=8] {'ep_0'}, dimensions={0} | all-to-all | bytes 786432 | tf_op jit(solution)/shard_map/all_to_all | solution.py:40
  93.2 0.1 reduce-scatter.2.cloned.1.call-start
  93.3 59.5 %all-gather.2.cloned.1.call-done = bf16[768,2048]{1,0:T(8,128)(2,1)} async-done(((bf16[768,256]{1,0:T(8,128)(2,1)}), bf16[768,2048]{1,0:T(8,128)(2,1)}) %all-gather.2.cloned.1.call-update) | async-done | bytes 3145744 | tf_op jit(solution)/shard_map/all_gather | solution.py:80
  152.8 3.8 %fusion.3 = f32[768,384]{1,0:T(8,128)S(1)} fusion(bf16[768,2048]{1,0:T(8,128)(2,1)} %all-gather.2.cloned.1.call-done, bf16[1,2048,384]{2,1,0:T(8,128)(2,1)S(1)} %copy-done.3), kind=kOutput, calls=%fused_computation.7 | convolution fusion | flops 1207959552 | bytes 5898240 | tf_op jit(solution)/shard_map/dot_general | solution.py:83
  156.6 1.8 fusion.8
  158.5 3.5 %convolution_convert_fusion = bf16[32,24,2048]{2,1,0:T(8,128)(2,1)} fusion(bf16[32,24,384]{2,1,0:T(8,128)(2,1)S(1)} %bitcast.48, bf16[1,384,2048]{2,1,0:T(8,128)(2,1)S(1)} %copy-done), kind=kOutput, calls=%fused_computation.3 | convolution fusion | flops 1209532416 | bytes 5308416 | tf_op jit(solution)/shard_map/dot_general | solution.py:86
  162.0 54.2 %reduce-scatter.2.cloned.1.call-done = bf16[32,24,256]{2,1,0:T(8,128)(2,1)} async-done(((bf16[32,24,2048]{2,1,0:T(8,128)(2,1)}), bf16[32,24,256]{2,1,0:T(8,128)(2,1)}) %reduce-scatter.2.cloned.1.call-update) | async-done | bytes 393232 | tf_op jit(solution)/shard_map/reduce_scatter | solution.py:88
  216.2 16.9 %all-to-all-start.3 = ((bf16[32,24,256]{2,1,0:T(8,128)(2,1)}), bf16[32,24,256]{2,1,0:T(8,128)(2,1)S(1)}, u32[]{:S(2)}, u32[]{:S(2)}) async-start(bf16[32,24,256]{2,1,0:T(8,128)(2,1)} %reduce-scatter.2.cloned.1.call-done), calls=%async_computation.4 | async-start | bytes 786432 | tf_op jit(solution)/shard_map/all_to_all | solution.py:91
  233.2 0.1 copy.21
  233.3 27.4 %all-to-all-done.3 = bf16[32,24,256]{2,1,0:T(8,128)(2,1)S(1)} async-done(((bf16[32,24,256]{2,1,0:T(8,128)(2,1)}), bf16[32,24,256]{2,1,0:T(8,128)(2,1)S(1)}, u32[]{:S(2)}, u32[]{:S(2)}) %all-to-all-start.3) | async-done | bytes 393248 | tf_op jit(solution)/shard_map/all_to_all | solution.py:91
  260.7 1.9 gather_fusion.1
  262.7 0.3 reshape.98
  262.9 1.4 multiply_reduce_fusion
  (27 shorter events, 0.3 us)
Async XLA Ops:
  6.5 152.0 %copy-start = (bf16[1,384,2048]{2,1,0:T(8,128)(2,1)S(1)}, bf16[1,384,2048]{2,1,0:T(8,128)(2,1)}, u32[]{:S(2)}) copy-start(bf16[1,384,2048]{2,1,0:T(8,128)(2,1)} %param.13) | copy-start | bytes 4718596
  8.3 15.0 %all-to-all-start = ((f32[8,256,1]{1,2,0:T(1,128)}), f32[8,256,1]{1,2,0:T(1,128)S(1)}, u32[]{:S(2)}, u32[]{:S(2)}) async-start(f32[8,256,1]{1,2,0:T(1,128)} %broadcast_in_dim.29), calls=%async_computation | async-start | bytes 16384 | tf_op jit(solution)/shard_map/all_to_all | solution.py:14
  16.2 136.6 %all-gather.2.cloned.1.call-start = ((), (), s32[]{:S(2)}) async-start(), calls=%async_computation.5 | async-start | bytes 3538944 | tf_op jit(solution)/shard_map/all_gather | solution.py:80
  27.1 125.6 %copy-start.3 = (bf16[1,2048,384]{2,1,0:T(8,128)(2,1)S(1)}, bf16[1,2048,384]{2,1,0:T(8,128)(2,1)}, u32[]{:S(2)}) copy-start(bf16[1,2048,384]{2,1,0:T(8,128)(2,1)} %param.11) | copy-start | bytes 4718596
  93.2 123.0 %reduce-scatter.2.cloned.1.call-start = ((), (), s32[]{:S(2)}) async-start(), calls=%async_computation.6 | async-start | bytes 3538944 | tf_op jit(solution)/shard_map/reduce_scatter | solution.py:88
  152.8 3.8 %copy-start.2 = (bf16[768,2048]{1,0:T(8,128)(2,1)S(1)}, bf16[768,2048]{1,0:T(8,128)(2,1)}, u32[]{:S(2)}) copy-start(bf16[768,2048]{1,0:T(8,128)(2,1)} %all-gather.2.cloned.1.call-done) | copy-start | bytes 9437188
  152.8 3.8 %copy-start.4 = (bf16[1,2048,384]{2,1,0:T(8,128)(2,1)S(1)}, bf16[1,2048,384]{2,1,0:T(8,128)(2,1)}, u32[]{:S(2)}) copy-start(bf16[1,2048,384]{2,1,0:T(8,128)(2,1)} %param.12) | copy-start | bytes 4718596
  162.0 71.2 %copy-start.1 = (f32[256,2]{0,1:T(2,128)S(1)}, f32[256,2]{0,1:T(2,128)}, u32[]{:S(2)}) copy-start(f32[256,2]{0,1:T(2,128)} %param.10) | copy-start | bytes 6148
  216.2 44.5 %all-to-all-start.3 = ((bf16[32,24,256]{2,1,0:T(8,128)(2,1)}), bf16[32,24,256]{2,1,0:T(8,128)(2,1)S(1)}, u32[]{:S(2)}, u32[]{:S(2)}) async-start(bf16[32,24,256]{2,1,0:T(8,128)(2,1)} %reduce-scatter.2.cloned.1.call-done), calls=%async_computation.4 | async-start | bytes 786432 | tf_op jit(solution)/shard_map/all_to_all | solution.py:91
Sparse Core Ops, SparseCore 0:
  93.3 59.4 all-gather.1
  162.2 54.0 reduce-scatter.1
where the time goes:
time: 272 us; the launch traced here: 271 us
  waiting for transfers between devices  141 us (52%)
  blocking collectives  65.9 us (24%)
  starting transfers between devices  24.9 us (9%)
  between operations  13.6 us (5%)
  local copies, waits for them, and re-layouts  10.6 us (4%)
  matrix products  9.14 us (3%)
  other arithmetic  5.77 us (2%)
    all_to_all x2, blocking collectives, moved_by_axis(): whole = lax.all_to_all(whole, axes[k], k, k, tiled=True)  65.9 us
    all_gather x1, waiting for transfers between devices, on_device(): col_piece = lax.all_gather(tok_rows, 'tp', axis=1, tiled=True)  59.5 us
    reduce_scatter x1, waiting for transfers between devices, on_device(): lax.psum_scatter(partial_value.astype(jnp.bfloat16), 'tp', scatter_dimens...  54.2 us
    all_to_all x1, waiting for transfers between devices, on_device(): lax.all_to_all(summed, EP, split_axis=0, concat_axis=0, tiled=True)  27.4 us
    all_to_all x1, starting transfers between devices, on_device(): lax.all_to_all(summed, EP, split_axis=0, concat_axis=0, tiled=True)  16.9 us
    all_to_all x1, starting transfers between devices, sent_to_all(): lax.all_to_all(jnp.broadcast_to(array[None], (count, *array.shape)), axis...  7.86 us
  transfers between devices with their start and end apart: 4, of which 3 were waited for; matrix products, arithmetic and copies ran while one was open for 3% of the time, Pallas kernels for 0%

commit v1 on v0

--- a/solution.py
+++ b/solution.py
@@ -77,7 +77,7 @@
     received = core_and_chips(buffer, ("ep_0", "ep_1"), (1, 0), 0, 0)
     source_count, item_count, col_count = received.shape
     tok_rows = received.reshape(-1, col_count)
-    col_piece = lax.all_gather(tok_rows, "tp", axis=1, tiled=True)
+    col_piece = jnp.concatenate(lax.all_gather(tok_rows, "tp"), axis=1)
     gate_rows = w_gate[0]
     up_rows = w_up[0]
     gate_part = jnp.dot(col_piece, gate_rows, preferred_element_type=jnp.float32)

time: 272 us -> 265 us (0.974)
  waiting for transfers between devices: 141 us -> 130 us
  local copies, waits for them, and re-layouts: 10.6 us -> 15.3 us
    all_gather x1, waiting for transfers between devices: 59.5 us -> 52.5 us  [on_device(): col_piece = jnp.concatenate(lax.all_gather(tok_rows, 'tp'), axis=1)]
    all_gather x0 -> x1, local copies, waits for them, and re-layouts: none -> 4.69 us  [on_device(): col_piece = jnp.concatenate(lax.all_gather(tok_rows, 'tp'), axis=1)]
    reduce_scatter x1, waiting for transfers between devices: 54.2 us -> 50.3 us  [on_device(): lax.psum_scatter(partial_value.astype(jnp.bfloat16), 'tp', scatter_dimens...]
where the time goes in v1:
time: 265 us
  waiting for transfers between devices  130 us (49%)
  blocking collectives  65.8 us (25%)
  starting transfers between devices  24.9 us (9%)
  local copies, waits for them, and re-layouts  15.3 us (6%)
  between operations  13.6 us (5%)
  matrix products  9.2 us (3%)
  other arithmetic  5.77 us (2%)
    all_to_all x2, blocking collectives, moved_by_axis(): whole = lax.all_to_all(whole, axes[k], k, k, tiled=True)  65.8 us
    all_gather x1, waiting for transfers between devices, on_device(): col_piece = jnp.concatenate(lax.all_gather(tok_rows, 'tp'), axis=1)  52.5 us
    reduce_scatter x1, waiting for transfers between devices, on_device(): lax.psum_scatter(partial_value.astype(jnp.bfloat16), 'tp', scatter_dimens...  50.3 us
    all_to_all x1, waiting for transfers between devices, on_device(): lax.all_to_all(summed, EP, split_axis=0, concat_axis=0, tiled=True)  27.4 us
    all_to_all x1, starting transfers between devices, on_device(): lax.all_to_all(summed, EP, split_axis=0, concat_axis=0, tiled=True)  16.9 us
    all_to_all x1, starting transfers between devices, sent_to_all(): lax.all_to_all(jnp.broadcast_to(array[None], (count, *array.shape)), axis...  7.86 us
  transfers between devices with their start and end apart: 4, of which 3 were waited for; matrix products, arithmetic and copies ran while one was open for 3% of the time, Pallas kernels for 0%

profile of v1, /device:TPU:65, one launch (start us, length us, event | category | flops | bytes accessed | tf_op | source)
XLA Modules:
  0.0 264.8 jit_solution(1449462710661547251)
XLA Ops:
  6.6 1.1 fusion.11
  7.7 0.6 broadcast_in_dim.29
  8.3 7.9 %all-to-all-start = ((f32[8,256,1]{1,2,0:T(1,128)}), f32[8,256,1]{1,2,0:T(1,128)S(1)}, u32[]{:S(2)}, u32[]{:S(2)}) async-start(f32[8,256,1]{1,2,0:T(1,128)} %broadcast_in_dim.29), calls=%async_computation | async-start | bytes 16384 | tf_op jit(solution)/shard_map/all_to_all | solution.py:14
  16.2 0.8 copy.22
  17.0 0.1 eq.29
  17.2 0.1 eq.25
  17.3 0.7 broadcast_multiply_fusion
  18.0 1.2 reduce-window.6
  19.2 0.2 slice_reduce_fusion
  19.5 0.1 copy.21
  19.6 0.1 mul.59
  19.8 0.1 fusion.16
  19.9 2.4 scatter_custom_fusion
  22.4 0.1 broadcast_in_dim.27
  22.5 0.8 dynamic_slice.3
  23.3 1.0 fusion.13
  24.3 2.7 %gather_fusion = bf16[768,256]{1,0:T(8,128)(2,1)S(1)} fusion(bf16[256,256]{1,0:T(8,128)(2,1)S(1)} %fusion.13, s32[1024]{0:T(1024)S(1)} %pad_clamp_fusion.1), kind=kCustom, calls=%fused_computation | custom fusion | bytes 789504 | tf_op jit(solution)/shard_map/jit(_take)/gather | solution.py:74
  27.0 0.2 copy_select_fusion
  27.1 41.2 %all_to_all.20 = bf16[16,2,1,24,256]{4,3,0,2,1:T(8,128)(2,1)S(1)} all-to-all(bf16[16,2,1,24,256]{4,3,0,2,1:T(8,128)(2,1)S(1)} %copy_select_fusion), channel_id=1, replica_groups=mesh['grp'=2,'ep_0'=16,'ep_1'=2,'tp'=8] {'ep_1'}, dimensions={1} | all-to-all | bytes 786432 | tf_op jit(solution)/shard_map/all_to_all | solution.py:40
  68.4 24.6 %all_to_all.21 = bf16[16,2,1,24,256]{4,3,1,2,0:T(8,128)(2,1)} all-to-all(bf16[16,2,1,24,256]{4,3,1,2,0:T(8,128)(2,1)S(1)} %copy.27), channel_id=1, replica_groups=mesh['grp'=2,'ep_0'=16,'ep_1'=2,'tp'=8] {'ep_0'}, dimensions={0} | all-to-all | bytes 786432 | tf_op jit(solution)/shard_map/all_to_all | solution.py:40
  93.1 52.5 %all-gather.2.cloned.1.call-done = bf16[8,768,256]{2,1,0:T(8,128)(2,1)} async-done(((bf16[1,768,256]{2,1,0:T(8,128)(2,1)}), bf16[8,768,256]{2,1,0:T(8,128)(2,1)}) %all-gather.2.cloned.1.call-update) | async-done | bytes 3145744 | tf_op jit(solution)/shard_map/all_gather | solution.py:80
  145.6 4.7 %copy.28 = bf16[8,768,256]{1,2,0:T(8,128)(2,1)} copy(bf16[8,768,256]{2,1,0:T(8,128)(2,1)} %all-gather.2.cloned.1.call-done) | data formatting | bytes 6291456 | tf_op jit(solution)/shard_map/all_gather | solution.py:80
  150.3 3.8 %fusion.3 = f32[768,384]{1,0:T(8,128)S(1)} fusion(bf16[768,2048]{0,1:T(8,128)(2,1)} %bitcast.46, bf16[1,2048,384]{2,1,0:T(8,128)(2,1)S(1)} %copy-done.2), kind=kOutput, calls=%fused_computation.7 | convolution fusion | flops 1207959552 | bytes 5898240 | tf_op jit(solution)/shard_map/dot_general | solution.py:83
  154.2 1.9 fusion.8
  156.1 3.5 %convolution_convert_fusion = bf16[32,24,2048]{2,1,0:T(8,128)(2,1)} fusion(bf16[32,24,384]{2,1,0:T(8,128)(2,1)S(1)} %bitcast.53, bf16[1,384,2048]{2,1,0:T(8,128)(2,1)S(1)} %copy-done), kind=kOutput, calls=%fused_computation.3 | convolution fusion | flops 1209532416 | bytes 5308416 | tf_op jit(solution)/shard_map/dot_general | solution.py:86
  159.6 50.3 %reduce-scatter.2.cloned.1.call-done = bf16[32,24,256]{2,1,0:T(8,128)(2,1)} async-done(((bf16[32,24,2048]{2,1,0:T(8,128)(2,1)}), bf16[32,24,256]{2,1,0:T(8,128)(2,1)}) %reduce-scatter.2.cloned.1.call-update) | async-done | bytes 393232 | tf_op jit(solution)/shard_map/reduce_scatter | solution.py:88
  209.9 16.9 %all-to-all-start.3 = ((bf16[32,24,256]{2,1,0:T(8,128)(2,1)}), bf16[32,24,256]{2,1,0:T(8,128)(2,1)S(1)}, u32[]{:S(2)}, u32[]{:S(2)}) async-start(bf16[32,24,256]{2,1,0:T(8,128)(2,1)} %reduce-scatter.2.cloned.1.call-done), calls=%async_computation.4 | async-start | bytes 786432 | tf_op jit(solution)/shard_map/all_to_all | solution.py:91
  226.8 0.1 copy.29
  227.0 27.4 %all-to-all-done.3 = bf16[32,24,256]{2,1,0:T(8,128)(2,1)S(1)} async-done(((bf16[32,24,256]{2,1,0:T(8,128)(2,1)}), bf16[32,24,256]{2,1,0:T(8,128)(2,1)S(1)}, u32[]{:S(2)}, u32[]{:S(2)}) %all-to-all-start.3) | async-done | bytes 393248 | tf_op jit(solution)/shard_map/all_to_all | solution.py:91
  254.4 1.9 gather_fusion.1
  256.3 0.3 reshape.106
  256.6 1.4 multiply_reduce_fusion
  (28 shorter events, 0.4 us)
Async XLA Ops:
  6.5 149.5 %copy-start = (bf16[1,384,2048]{2,1,0:T(8,128)(2,1)S(1)}, bf16[1,384,2048]{2,1,0:T(8,128)(2,1)}, u32[]{:S(2)}) copy-start(bf16[1,384,2048]{2,1,0:T(8,128)(2,1)} %param.13) | copy-start | bytes 4718596
  8.3 15.0 %all-to-all-start = ((f32[8,256,1]{1,2,0:T(1,128)}), f32[8,256,1]{1,2,0:T(1,128)S(1)}, u32[]{:S(2)}, u32[]{:S(2)}) async-start(f32[8,256,1]{1,2,0:T(1,128)} %broadcast_in_dim.29), calls=%async_computation | async-start | bytes 16384 | tf_op jit(solution)/shard_map/all_to_all | solution.py:14
  16.2 129.4 %all-gather.2.cloned.1.call-start = ((), (), s32[]{:S(2)}) async-start(), calls=%async_computation.5 | async-start | bytes 3538944 | tf_op jit(solution)/shard_map/all_gather | solution.py:80
  93.0 57.2 %copy-start.2 = (bf16[1,2048,384]{2,1,0:T(8,128)(2,1)S(1)}, bf16[1,2048,384]{2,1,0:T(8,128)(2,1)}, u32[]{:S(2)}) copy-start(bf16[1,2048,384]{2,1,0:T(8,128)(2,1)} %param.11) | copy-start | bytes 4718596
  93.1 116.9 %reduce-scatter.2.cloned.1.call-start = ((), (), s32[]{:S(2)}) async-start(), calls=%async_computation.6 | async-start | bytes 3538944 | tf_op jit(solution)/shard_map/reduce_scatter | solution.py:88
  150.3 3.9 %copy-start.1 = (bf16[8,768,256]{1,2,0:T(8,128)(2,1)S(1)}, bf16[8,768,256]{1,2,0:T(8,128)(2,1)}, u32[]{:S(2)}) copy-start(bf16[8,768,256]{1,2,0:T(8,128)(2,1)} %copy.28) | copy-start | bytes 9437188
  150.3 3.9 %copy-start.4 = (bf16[1,2048,384]{2,1,0:T(8,128)(2,1)S(1)}, bf16[1,2048,384]{2,1,0:T(8,128)(2,1)}, u32[]{:S(2)}) copy-start(bf16[1,2048,384]{2,1,0:T(8,128)(2,1)} %param.12) | copy-start | bytes 4718596
  159.5 67.3 %copy-start.3 = (f32[256,2]{0,1:T(2,128)S(1)}, f32[256,2]{0,1:T(2,128)}, u32[]{:S(2)}) copy-start(f32[256,2]{0,1:T(2,128)} %param.10) | copy-start | bytes 6148
  209.9 44.4 %all-to-all-start.3 = ((bf16[32,24,256]{2,1,0:T(8,128)(2,1)}), bf16[32,24,256]{2,1,0:T(8,128)(2,1)S(1)}, u32[]{:S(2)}, u32[]{:S(2)}) async-start(bf16[32,24,256]{2,1,0:T(8,128)(2,1)} %reduce-scatter.2.cloned.1.call-done), calls=%async_computation.4 | async-start | bytes 786432 | tf_op jit(solution)/shard_map/all_to_all | solution.py:91
Sparse Core Ops, SparseCore 0:
  93.2 52.3 all-gather.1
  159.7 50.1 reduce-scatter.1
